TPU v7x, 768 devices: a whole 4x8x12 slice. The times are simulated.
768 devices in a mesh: ep: 24 (over z, core), tp: 32 (over y, x).
Axes of the slice: x: 4, y: 8, z: 12, core: 2. Of those that a mesh axis runs over, the one named last changes fastest.
Arguments:
- tokens: bfloat16 [6144, 2048], P('ep'), may hold values from -6 to 6
- norm_gain: float32 [2048], replicated, may hold values from 0.1 to 1.9
- expert_ids: int32 [6144, 2], P('ep'), may hold values from 0 to 23, all different within a row; in each aligned block of 256 rows (0 to 255, 256 to 511, ...) at most 32 rows name the same one
- routing_weight: float32 [6144, 2], P('ep'), may hold values from 0.1 to 1
- expert_gate: bfloat16 [24, 2048, 5632], P('ep', None, 'tp'), may hold values from -0.125 to 0.125
- expert_up: bfloat16 [24, 2048, 5632], P('ep', None, 'tp'), may hold values from -0.125 to 0.125
- expert_down: bfloat16 [24, 5632, 2048], P('ep', 'tp'), may hold values from -0.078125 to 0.078125
- dense_gate_w: bfloat16 [2048, 1024], P(None, 'tp'), may hold values from -0.125 to 0.125
- dense_up_w: bfloat16 [2048, 1024], P(None, 'tp'), may hold values from -0.125 to 0.125
- dense_down_w: bfloat16 [1024, 2048], P('tp'), may hold values from -0.1875 to 0.1875
- dense_gate: float32 [2048], P('tp'), may hold values from -3 to 3
Outputs:
- layer_out: bfloat16 [6144, 2048], P('ep', 'tp')
Inputs may be any that keep to these rules, and one draw needn't show every extreme that they name: `expert_ids`: within the 256 rows of one device along ep, each row names two different experts and no expert is named by more than 32 rows; some expert is named by exactly 32 rows.
All inputs are finite; a program needn't handle non-finite values.
Results may differ from a plain program's by a relative error of at most 0.017.
Values may be sent and summed in bfloat16 or wider, within the bound.
No kernel may reach another device: no remote copies, remote signals or barrier semaphores. Data moves between devices by JAX's collectives and lax.ppermute only.
A program may use at most 64 MiB of HBM per device.

v0:
```python
import jax
import jax.numpy as jnp
from jax import lax
from jax.sharding import Mesh
from jax.sharding import PartitionSpec as P

TP = ("tp_0", "tp_1")


EPSILON = 1e-06


def gathered_by_axis(value, axes, dim):
    if not axes:
        return value
    nearer = lax.all_gather(value, axes[-1], axis=dim, tiled=True)
    return gathered_by_axis(nearer, axes[:-1], dim)


def in_blocks(value, dim, count):
    before, after = (value.shape[:dim], value.shape[dim + 1 :])
    return jnp.moveaxis(value.reshape(*before, count, -1, *after), dim, 0)


def sum_at_owner(value, axis, dim):
    blocks = in_blocks(value, dim, lax.axis_size(axis))
    arrived = lax.all_to_all(blocks, axis, split_axis=0, concat_axis=0, tiled=True)
    return arrived.astype(jnp.float32).sum(axis=0)


def sum_by_axis(terms, axes):
    so_far = terms.astype(jnp.bfloat16)
    for axis in axes:
        so_far = lax.psum_scatter(so_far, axis, scatter_dimension=0, tiled=True)
    return so_far.astype(jnp.float32)


def positions(block_ids, experts, capacity):
    flat_ids = block_ids.reshape(-1)
    one_hot = (flat_ids[:, None] == jnp.arange(experts, dtype=jnp.int32)[None, :]).astype(jnp.int32)
    earlier = jnp.cumsum(one_hot, axis=0) - one_hot
    return flat_ids * capacity + jnp.sum(earlier * one_hot, axis=1)


def transposed_term(hidden, down_w):
    return lax.dot_general(
        down_w, hidden, (((0,), (1,)), ((), ())), preferred_element_type=jnp.float32
    )


def local(
    tokens,
    norm_gain,
    expert_ids,
    routing_weight,
    expert_gate,
    expert_up,
    expert_down,
    dense_gate_w,
    dense_up_w,
    dense_down_w,
    dense_gate,
):
    experts = lax.axis_size("ep")
    group_tokens, model_width = tokens.shape
    capacity = 3 * group_tokens // experts
    slots_all = experts * capacity
    part_rows = model_width // lax.axis_size(TP)
    values = tokens.astype(jnp.float32)
    factor = lax.rsqrt(jnp.mean(values * values, axis=-1, keepdims=True) + EPSILON)
    normed = (values * factor * norm_gain[None, :]).astype(jnp.bfloat16)
    places = positions(expert_ids, experts, capacity)
    token_no = jnp.arange(2 * group_tokens, dtype=jnp.int32) // 2 + 1
    sources = jnp.zeros((slots_all,), jnp.int32).at[places].set(token_no)
    padded = jnp.concatenate([jnp.zeros((1, model_width), jnp.bfloat16), normed], axis=0)
    gate_w = expert_gate[0]
    up_w = expert_up[0]
    down_w = expert_down[0]
    first_col = lax.axis_index(TP) * part_rows
    column_part = lax.dynamic_slice_in_dim(padded, first_col, part_rows, 1)
    outgoing = column_part[sources].reshape(experts, capacity, part_rows)
    landed = lax.all_to_all(outgoing, "ep", split_axis=0, concat_axis=0, tiled=True)
    portion = gathered_by_axis(landed, TP, 2)
    columns = portion.reshape(slots_all, portion.shape[2])
    gate_act = jnp.dot(columns, gate_w, preferred_element_type=jnp.float32)
    up_act = jnp.dot(columns, up_w, preferred_element_type=jnp.float32)
    hidden = (jax.nn.silu(gate_act) * up_act).astype(jnp.bfloat16)
    dense_gate_act = jnp.dot(normed, dense_gate_w, preferred_element_type=jnp.float32)
    dense_up_act = jnp.dot(normed, dense_up_w, preferred_element_type=jnp.float32)
    dense_hidden = (jax.nn.silu(dense_gate_act) * dense_up_act).astype(jnp.bfloat16)
    dense_out = sum_at_owner(
        transposed_term(dense_hidden, dense_down_w).astype(jnp.bfloat16), TP, 0
    )
    expert_out = sum_by_axis(transposed_term(hidden, down_w), TP)
    expert_half = expert_out.astype(jnp.bfloat16).reshape(part_rows, experts, capacity)
    returned = lax.all_to_all(expert_half, "ep", split_axis=1, concat_axis=1, tiled=True).reshape(
        part_rows, slots_all
    )
    picked = (
        jnp.take(returned, places, axis=1).astype(jnp.float32).reshape(part_rows, group_tokens, 2)
    )
    routed = jnp.sum(picked * routing_weight[None, :, :], axis=2)
    gate_factor = jax.nn.sigmoid(dense_gate)[:, None]
    return (routed + gate_factor * dense_out).T.astype(jnp.bfloat16)


def solution(mesh):
    finer = Mesh(mesh.devices.reshape(mesh.shape["ep"], 8, 4), ("ep", "tp_0", "tp_1"))
    in_specs = (
        P("ep", None),
        P(),
        P("ep", None),
        P("ep", None),
        P("ep", None, TP),
        P("ep", None, TP),
        P("ep", TP, None),
        P(None, TP),
        P(None, TP),
        P(TP, None),
        P(TP),
    )
    out_specs = P("ep", TP)
    return jax.shard_map(local, mesh=finer, in_specs=in_specs, out_specs=out_specs, check_vma=False)
```

profile of v0, /device:TPU:1, one launch (start us, length us, event | category | flops | bytes accessed | tf_op | source)
XLA Modules:
  0.0 259.8 jit_solution(18381356315975657672)
XLA Ops:
  8.4 1.5 fusion.2
  10.2 1.2 reduce-window.6
  11.8 2.4 scatter_custom_fusion
  14.3 1.5 fusion.4
  15.9 1.9 gather_fusion
  18.0 27.5 %all_to_all.15 = bf16[24,2,1024]{2,1,0:T(2,128)(2,1)S(1)} all-to-all(bf16[24,2,1024]{2,1,0:T(2,128)(2,1)S(1)} %reshape.125), channel_id=1, replica_groups=mesh['ep'=24,'tp_0'=8,'tp_1'=4] {'ep'}, dimensions={0} | all-to-all | bytes 196608 | tf_op jit(solution)/shard_map/all_to_all | solution.py:82
  45.6 1.0 copy.53
  46.6 16.2 %all_gather.6 = bf16[24,32,256]{1,0,2:T(8,128)(2,1)S(1)} all-gather(bf16[24,32,64]{1,0,2:T(8,128)(2,1)} %copy.53), channel_id=1, replica_groups=mesh['ep'=24,'tp_0'=8,'tp_1'=4] {'tp_1'}, dimensions={2}, use_global_device_ids=true | all-gather | bytes 491520 | tf_op jit(solution)/shard_map/all_gather | solution.py:16
  62.8 1.6 copy.54
  64.4 52.2 %all-gather.2.cloned.1.call-done = bf16[24,32,2048]{2,1,0:T(8,128)(2,1)} async-done(((bf16[24,32,256]{2,1,0:T(8,128)(2,1)}), bf16[24,32,2048]{2,1,0:T(8,128)(2,1)}) %all-gather.2.cloned.1.call-update) | async-done | bytes 3145744 | tf_op jit(solution)/shard_map/all_gather | solution.py:16
  116.6 3.2 %fusion.10 = f32[768,176]{0,1:T(8,128)S(1)} fusion(bf16[768,2048]{1,0:T(8,128)(2,1)} %bitcast.64, bf16[1,2048,176]{1,2,0:T(8,128)(2,1)} %param.15), kind=kOutput, calls=%fused_computation.20 | convolution fusion | flops 553648128 | bytes 4407296 | tf_op jit(solution)/shard_map/dot_general | solution.py:85
  119.9 6.0 %fusion = bf16[2048,768]{0,1:T(8,128)(2,1)} fusion(bf16[768,2048]{1,0:T(8,128)(2,1)} %bitcast.65, bf16[1,176,2048]{2,1,0:T(8,128)(2,1)S(1)} %copy-done, bf16[1,2048,176]{1,2,0:T(8,128)(2,1)S(1)} %copy-done.6, f32[768,176]{0,1:T(8,128)S(1)} %fusion.10), kind=kOutput, calls=%fused_computation.4 | convolution fusion | flops 1109680128 | bytes 8273920 | tf_op jit(solution)/shard_map/dot_general | solution.py:46
  126.0 0.9 copy-done.1
  127.3 1.4 fusion.1
  128.7 1.3 copy.56
  130.0 6.5 %all-to-all-start.2 = ((bf16[32,64,256]{2,1,0:T(8,128)(2,1)}), bf16[32,64,256]{2,1,0:T(8,128)(2,1)S(1)}, u32[]{:S(2)}, u32[]{:S(2)}) async-start(bf16[32,64,256]{2,1,0:T(8,128)(2,1)} %bitcast.56), calls=%async_computation.3 | async-start | bytes 2097152 | tf_op jit(solution)/shard_map/all_to_all | solution.py:27
  136.5 56.0 %reduce-scatter.5.cloned.1.call-done = bf16[256,768]{0,1:T(8,128)(2,1)} async-done(((bf16[2048,768]{0,1:T(8,128)(2,1)}), bf16[256,768]{0,1:T(8,128)(2,1)}) %reduce-scatter.5.cloned.1.call-update) | async-done | bytes 393232 | tf_op jit(solution)/shard_map/reduce_scatter | solution.py:34
  192.6 1.9 copy.59
  194.7 29.1 %reduce-scatter.7.cloned.1.call-done = bf16[64,768]{1,0:T(8,128)(2,1)} async-done(((bf16[256,768]{1,0:T(8,128)(2,1)}), bf16[64,768]{1,0:T(8,128)(2,1)}) %reduce-scatter.7.cloned.1.call-update) | async-done | bytes 98320
  223.9 1.1 copy.60
  225.7 12.8 %all-to-all-start.1 = ((bf16[24,2,1024]{2,1,0:T(2,128)(2,1)}), bf16[24,2,1024]{2,1,0:T(2,128)(2,1)S(1)}, u32[]{:S(2)}, u32[]{:S(2)}) async-start(bf16[24,2,1024]{2,1,0:T(2,128)(2,1)} %reshape.127), calls=%async_computation.2 | async-start | bytes 196608 | tf_op jit(solution)/shard_map/all_to_all | solution.py:96
  239.1 10.4 %all-to-all-done.1 = bf16[24,2,1024]{2,1,0:T(2,128)(2,1)S(1)} async-done(((bf16[24,2,1024]{2,1,0:T(2,128)(2,1)}), bf16[24,2,1024]{2,1,0:T(2,128)(2,1)S(1)}, u32[]{:S(2)}, u32[]{:S(2)}) %all-to-all-start.1) | async-done | bytes 98336 | tf_op jit(solution)/shard_map/all_to_all | solution.py:96
  249.7 1.3 gather_fusion.1
  251.1 1.5 multiply_reduce_fusion
  (55 shorter events, 6.1 us)
Async XLA Ops:
  6.5 113.3 %copy-start = (bf16[1,176,2048]{2,1,0:T(8,128)(2,1)S(1)}, bf16[1,176,2048]{2,1,0:T(8,128)(2,1)}, u32[]{:S(2)}) copy-start(bf16[1,176,2048]{2,1,0:T(8,128)(2,1)} %param.17) | copy-start | bytes 2162692
  6.5 110.1 %all-gather.2.cloned.1.call-start = ((), (), s32[]{:S(2)}) async-start(), calls=%async_computation.5 | async-start | bytes 3538944 | tf_op jit(solution)/shard_map/all_gather | solution.py:16
  64.4 55.5 %copy-start.6 = (bf16[1,2048,176]{1,2,0:T(8,128)(2,1)S(1)}, bf16[1,2048,176]{1,2,0:T(8,128)(2,1)}, u32[]{:S(2)}) copy-start(bf16[1,2048,176]{1,2,0:T(8,128)(2,1)} %param.16) | copy-start | bytes 2162692
  64.4 128.2 %reduce-scatter.5.cloned.1.call-start = ((), (), s32[]{:S(2)}) async-start(), calls=%async_computation.6 | async-start | bytes 3538944 | tf_op jit(solution)/shard_map/reduce_scatter | solution.py:34
  125.9 0.9 copy-start.1
  125.9 1.3 copy-start.2
  125.9 1.3 copy-start.3
  128.6 66.1 %copy-start.4 = (s32[256,2]{0,1:T(2,128)S(1)}, s32[256,2]{0,1:T(2,128)}, u32[]{:S(2)}) copy-start(s32[256,2]{0,1:T(2,128)} %param.13) | copy-start | bytes 6148
  128.7 109.9 %copy-start.7 = (f32[64]{0:T(128)S(1)}, f32[64]{0:T(128)}, u32[]{:S(2)}) copy-start(f32[64]{0:T(128)} %param.21) | copy-start | bytes 772
  128.7 110.0 %copy-start.5 = (f32[256,2]{0,1:T(2,128)S(1)}, f32[256,2]{0,1:T(2,128)}, u32[]{:S(2)}) copy-start(f32[256,2]{0,1:T(2,128)} %param.14) | copy-start | bytes 6148
  130.0 95.7 %all-to-all-start.2 = ((bf16[32,64,256]{2,1,0:T(8,128)(2,1)}), bf16[32,64,256]{2,1,0:T(8,128)(2,1)S(1)}, u32[]{:S(2)}, u32[]{:S(2)}) async-start(bf16[32,64,256]{2,1,0:T(8,128)(2,1)} %bitcast.56), calls=%async_computation.3 | async-start | bytes 2097152 | tf_op jit(solution)/shard_map/all_to_all | solution.py:27
  136.5 87.4 %reduce-scatter.7.cloned.1.call-start = ((), (), s32[]{:S(2)}) async-start(), calls=%async_computation.7 | async-start | bytes 491520
  225.7 23.8 %all-to-all-start.1 = ((bf16[24,2,1024]{2,1,0:T(2,128)(2,1)}), bf16[24,2,1024]{2,1,0:T(2,128)(2,1)S(1)}, u32[]{:S(2)}, u32[]{:S(2)}) async-start(bf16[24,2,1024]{2,1,0:T(2,128)(2,1)} %reshape.127), calls=%async_computation.2 | async-start | bytes 196608 | tf_op jit(solution)/shard_map/all_to_all | solution.py:96
Sparse Core Ops, SparseCore 0:
  64.5 52.0 all-gather.1
  126.1 66.4 reduce-scatter.4
  195.7 28.1 reduce-scatter.6
where the time goes:
time: 260 us
  waiting for transfers between devices  148 us (57%)
  blocking collectives  43.7 us (17%)
  starting transfers between devices  19.3 us (7%)
  local copies, waits for them, and re-layouts  17.8 us (7%)
  between operations  13.4 us (5%)
  matrix products  11.1 us (4%)
  other arithmetic  6.8 us (3%)
    reduce_scatter x1, waiting for transfers between devices, sum_by_axis(): so_far = lax.psum_scatter(so_far, axis, scatter_dimension=0, tiled=True)  56 us
    all_gather x1, waiting for transfers between devices, gathered_by_axis(): nearer = lax.all_gather(value, axes[-1], axis=dim, tiled=True)  52.2 us
    unnamed x4, waiting for transfers between devices  29.2 us
    all_to_all x1, blocking collectives, local(): lax.all_to_all(outgoing, 'ep', split_axis=0, concat_axis=0, tiled=True)  27.5 us
    all_gather x1, blocking collectives, gathered_by_axis(): nearer = lax.all_gather(value, axes[-1], axis=dim, tiled=True)  16.2 us
    all_to_all x1, starting transfers between devices, local(): lax.all_to_all(expert_half, 'ep', split_axis=1, concat_axis=1, tiled=True)  12.8 us
    all_to_all x1, waiting for transfers between devices, local(): lax.all_to_all(expert_half, 'ep', split_axis=1, concat_axis=1, tiled=True)  10.4 us
    dot_general x2, matrix products, transposed_term(): lax.dot_general(down_w, hidden, (((0,), (1,)), ((), ())), preferred_eleme...  7.4 us
  transfers between devices with their start and end apart: 5, of which 4 were waited for; matrix products, arithmetic and copies ran while one was open for 3% of the time, Pallas kernels for 0%

commit v1 on v0

v1 whole, which is shorter than its diff:
```python
import jax
import jax.numpy as jnp
from jax import lax
from jax.sharding import Mesh
from jax.sharding import PartitionSpec as P

TP = ("tp_0", "tp_1")

EPSILON = 1e-06


def positions(block_ids, experts, capacity):
    flat_ids = block_ids.reshape(-1)
    one_hot = (flat_ids[:, None] == jnp.arange(experts, dtype=jnp.int32)[None, :]).astype(jnp.int32)
    earlier = jnp.cumsum(one_hot, axis=0) - one_hot
    return flat_ids * capacity + jnp.sum(earlier * one_hot, axis=1)


def exchange(blocks, axis):
    return lax.all_to_all(blocks, axis, split_axis=0, concat_axis=0, tiled=True)


def copies_from_all(value, axis):
    count = lax.axis_size(axis)
    sent = jnp.broadcast_to(value[None], (count, *value.shape))
    return exchange(sent, axis).reshape(count * value.shape[0], *value.shape[1:])


def sum_at_owner(value, axis):
    count = lax.axis_size(axis)
    blocks = value.reshape(count, value.shape[0] // count, *value.shape[1:])
    return exchange(blocks, axis).astype(jnp.float32).sum(axis=0)


def columns_by_owner(weight, far, near):
    rows, width = weight.shape
    part = width // (far * near)
    return weight.reshape(rows, far, near, part).transpose(0, 2, 1, 3).reshape(rows, width)


def contract_first(left, right):
    return lax.dot_general(left, right, (((0,), (0,)), ((), ())), preferred_element_type=jnp.float32)


def local(
    tokens,
    norm_gain,
    expert_ids,
    routing_weight,
    expert_gate,
    expert_up,
    expert_down,
    dense_gate_w,
    dense_up_w,
    dense_down_w,
    dense_gate,
):
    experts = lax.axis_size("ep")
    far, near = lax.axis_size("tp_0"), lax.axis_size("tp_1")
    group_tokens, model_width = tokens.shape
    capacity = 3 * group_tokens // experts
    slots_all = experts * capacity
    part = model_width // (far * near)
    values = tokens.astype(jnp.float32)
    factor = lax.rsqrt(jnp.mean(values * values, axis=-1, keepdims=True) + EPSILON)
    normed = (values * factor * norm_gain[None, :]).astype(jnp.bfloat16)
    places = positions(expert_ids, experts, capacity)

    token_no = jnp.arange(2 * group_tokens, dtype=jnp.int32) // 2 + 1
    sources = jnp.zeros((slots_all,), jnp.int32).at[places].set(token_no)
    padded = jnp.concatenate([jnp.zeros((1, model_width), jnp.bfloat16), normed], axis=0)
    first = (lax.axis_index("tp_1") * far + lax.axis_index("tp_0")) * part
    column_part = lax.dynamic_slice_in_dim(padded, first, part, 1)
    outgoing = column_part[sources].reshape(experts, capacity * part // 128, 128)
    landed = exchange(outgoing, "ep")
    landed = landed.reshape(slots_all, part).T
    rows_t = copies_from_all(copies_from_all(landed, "tp_0"), "tp_1")

    gate_act = contract_first(expert_gate[0], rows_t)
    up_act = contract_first(expert_up[0], rows_t)
    hidden = (jax.nn.silu(gate_act) * up_act).astype(jnp.bfloat16)
    dense_gate_act = lax.dot_general(
        dense_gate_w, normed, (((0,), (1,)), ((), ())), preferred_element_type=jnp.float32
    )
    dense_up_act = lax.dot_general(
        dense_up_w, normed, (((0,), (1,)), ((), ())), preferred_element_type=jnp.float32
    )
    dense_hidden = (jax.nn.silu(dense_gate_act) * dense_up_act).astype(jnp.bfloat16)

    both_hidden = jnp.concatenate(
        [
            jnp.pad(hidden, ((0, 0), (0, group_tokens))),
            jnp.pad(dense_hidden, ((0, 0), (slots_all, 0))),
        ],
        axis=0,
    )
    both_down = columns_by_owner(jnp.concatenate([expert_down[0], dense_down_w], axis=0), far, near)
    partial = contract_first(both_down, both_hidden).astype(jnp.bfloat16)
    over_near = sum_at_owner(partial, "tp_1").astype(jnp.bfloat16)
    total = sum_at_owner(over_near, "tp_0")
    dense_out = total[:, slots_all:]
    expert_out = total[:, :slots_all].astype(jnp.bfloat16).reshape(part, experts, capacity)
    going_back = expert_out.transpose(1, 2, 0).reshape(experts, capacity * part // 128, 128)
    returned = exchange(going_back, "ep").reshape(slots_all, part)

    picked = jnp.take(returned, places, axis=0).astype(jnp.float32)
    picked = picked.reshape(group_tokens, 2, part)
    routed = jnp.sum(picked * routing_weight[:, :, None], axis=1)
    gate_factor = jax.nn.sigmoid(dense_gate)[None, :]
    return (routed + gate_factor * dense_out.T).astype(jnp.bfloat16)


def solution(mesh):
    finer = Mesh(mesh.devices.reshape(mesh.shape["ep"], 8, 4), ("ep", "tp_0", "tp_1"))
    in_specs = (
        P("ep", None),
        P(),
        P("ep", None),
        P("ep", None),
        P("ep", None, TP),
        P("ep", None, TP),
        P("ep", TP, None),
        P(None, TP),
        P(None, TP),
        P(TP, None),
        P(TP),
    )
    out_specs = P("ep", TP)
    return jax.shard_map(local, mesh=finer, in_specs=in_specs, out_specs=out_specs, check_vma=False)
```

time: 260 us -> 228 us (0.88)
  waiting for transfers between devices: 148 us -> 69.7 us
  blocking collectives: 43.7 us -> 105 us
  between operations: 13.4 us -> 0.34 us
  other arithmetic: 6.8 us -> 12.1 us
  local copies, waits for them, and re-layouts: 17.8 us -> 13.3 us
  matrix products: 11.1 us -> 7.55 us
    all_to_all x1 -> x3, blocking collectives: 27.5 us -> 105 us  [exchange(): return lax.all_to_all(blocks, axis, split_axis=0, concat_axis=0, tiled=True)]
    all_to_all x2 -> x3, waiting for transfers between devices: 10.4 us -> 69.7 us  [exchange(): return lax.all_to_all(blocks, axis, split_axis=0, concat_axis=0, tiled=True)]
    reduce_scatter x1 -> x0, waiting for transfers between devices: 56 us -> none  [sum_by_axis(): so_far = lax.psum_scatter(so_far, axis, scatter_dimension=0, tiled=True)]
    all_gather x1 -> x0, waiting for transfers between devices: 52.2 us -> none  [gathered_by_axis(): nearer = lax.all_gather(value, axes[-1], axis=dim, tiled=True)]
    unnamed x4 -> x0, waiting for transfers between devices: 29.2 us -> none
    all_gather x1 -> x0, blocking collectives: 16.2 us -> none  [gathered_by_axis(): nearer = lax.all_gather(value, axes[-1], axis=dim, tiled=True)]
    reduce_sum x2 -> x3, other arithmetic: 1.62 us -> 6.03 us  [the longest x2 4.57 us: sum_at_owner(): return exchange(blocks, axis).astype(jnp.float32).sum(axis=0)]
    dot_general x4 -> x5, matrix products: 11.1 us -> 7.55 us  [the longest x3 6.71 us: contract_first(): lax.dot_general(left, right, (((0,), (0,)), ((), ())), preferred_element_...]
  transfers between devices with their start and end apart: 5 -> 3, of which waited for: 4 -> 3; matrix products, arithmetic and copies ran while one was open for 3% -> 2% of each run, Pallas kernels for 0% -> 0%
where the time goes in v1:
time: 228 us; the launch traced here: 227 us
  blocking collectives  105 us (46%)
  waiting for transfers between devices  69.7 us (31%)
  starting transfers between devices  18.8 us (8%)
  local copies, waits for them, and re-layouts  13.3 us (6%)
  other arithmetic  12.1 us (5%)
  matrix products  7.55 us (3%)
    all_to_all x3, blocking collectives, exchange(): return lax.all_to_all(blocks, axis, split_axis=0, concat_axis=0, tiled=True)  105 us
    all_to_all x3, waiting for transfers between devices, exchange(): return lax.all_to_all(blocks, axis, split_axis=0, concat_axis=0, tiled=True)  69.7 us
    all_to_all x3, starting transfers between devices, exchange(): return lax.all_to_all(blocks, axis, split_axis=0, concat_axis=0, tiled=True)  18.8 us
    dot_general x3, matrix products, contract_first(): lax.dot_general(left, right, (((0,), (0,)), ((), ())), preferred_element_...  6.71 us
    reduce_sum x2, other arithmetic, sum_at_owner(): return exchange(blocks, axis).astype(jnp.float32).sum(axis=0)  4.57 us
  transfers between devices with their start and end apart: 3, of which 3 were waited for; matrix products, arithmetic and copies ran while one was open for 2% of the time, Pallas kernels for 0%

profile of v1, /device:TPU:1, one launch (start us, length us, event | category | flops | bytes accessed | tf_op | source)
XLA Modules:
  0.0 227.0 jit_solution(13974879647651571839)
XLA Ops:
  0.0 0.9 copy.47
  1.9 1.5 fusion
  3.4 1.2 reduce-window.6
  5.2 2.4 %scatter_custom_fusion = s32[768]{0:T(1024)S(1)} fusion(s32[512]{0:T(512)S(1)} %bitcast.79, s32[512]{0:T(512)S(1)} %fusion.25, s32[]{:T(128)} %constant.33.clone.1), kind=kCustom, calls=%fused_computation.60 | custom fusion | bytes 3076 | tf_op jit(solution)/shard_map/scatter | solution.py:70
  7.7 1.5 fusion.2
  9.4 1.9 gather_fusion
  11.4 27.5 %all_to_all.30 = bf16[24,16,128]{2,1,0:T(8,128)(2,1)S(1)} all-to-all(bf16[24,16,128]{2,1,0:T(8,128)(2,1)S(1)} %reshape.109), channel_id=1, replica_groups=mesh['ep'=24,'tp_0'=8,'tp_1'=4] {'ep'}, dimensions={0} | all-to-all | bytes 196608 | tf_op jit(solution)/shard_map/all_to_all | solution.py:20
  39.2 28.4 %all_to_all.31 = bf16[8,64,768]{2,1,0:T(8,128)(2,1)S(1)} all-to-all(bf16[8,64,768]{2,1,0:T(8,128)(2,1)S(1)} %broadcast_in_dim.20), channel_id=1, replica_groups=mesh['ep'=24,'tp_0'=8,'tp_1'=4] {'tp_0'}, dimensions={0} | all-to-all | bytes 1572864 | tf_op jit(solution)/shard_map/all_to_all | solution.py:20
  67.6 1.9 broadcast_in_dim.37
  69.5 4.8 %all-to-all-start.2 = ((bf16[4,512,768]{2,1,0:T(8,128)(2,1)}), bf16[4,512,768]{2,1,0:T(8,128)(2,1)}, u32[]{:S(2)}, u32[]{:S(2)}) async-start(bf16[4,512,768]{2,1,0:T(8,128)(2,1)} %broadcast_in_dim.37), calls=%async_computation.2 | async-start | bytes 6291456 | tf_op jit(solution)/shard_map/all_to_all | solution.py:20
  74.8 1.2 copy.53
  77.4 32.3 %all-to-all-done.2 = bf16[4,512,768]{2,1,0:T(8,128)(2,1)} async-done(((bf16[4,512,768]{2,1,0:T(8,128)(2,1)}), bf16[4,512,768]{2,1,0:T(8,128)(2,1)}, u32[]{:S(2)}, u32[]{:S(2)}) %all-to-all-start.2) | async-done | bytes 3145760 | tf_op jit(solution)/shard_map/all_to_all | solution.py:20
  109.7 2.6 %convolution_bitcast_fusion.1 = f32[176,768]{1,0:T(8,128)S(1)} fusion(bf16[2048,768]{1,0:T(8,128)(2,1)} %bitcast.9, bf16[1,2048,176]{1,2,0:T(8,128)(2,1)S(1)} %copy-done), kind=kOutput, calls=%fused_computation.11 | convolution fusion | flops 553648128 | bytes 4407296 | tf_op jit(solution)/shard_map/dot_general | solution.py:42
  112.4 2.9 %fusion.4 = bf16[176,768]{1,0:T(8,128)(2,1)S(1)} fusion(bf16[2048,768]{1,0:T(8,128)(2,1)} %bitcast.9, bf16[1,2048,176]{1,2,0:T(8,128)(2,1)} %param.16, f32[176,768]{1,0:T(8,128)S(1)} %convolution_bitcast_fusion.1), kind=kOutput, calls=%fused_computation.13 | convolution fusion | flops 554459136 | bytes 4677632 | tf_op jit(solution)/shard_map/dot_general | solution.py:42
  115.2 1.2 convolution_convert_fusion
  116.5 49.2 %all_to_all.32 = bf16[4,512,1024]{2,1,0:T(8,128)(2,1)} all-to-all(bf16[4,512,1024]{2,1,0:T(8,128)(2,1)S(1)} %bitcast.70), channel_id=1, replica_groups=mesh['ep'=24,'tp_0'=8,'tp_1'=4] {'tp_1'}, dimensions={0} | all-to-all | bytes 8388608 | tf_op jit(solution)/shard_map/all_to_all | solution.py:20
  165.7 4.4 %reduce_sum.56 = bf16[512,1024]{1,0:T(8,128)(2,1)} reduce(bf16[4,512,1024]{2,1,0:T(8,128)(2,1)} %all_to_all.32, bf16[]{:T(256)} %constant.64.clone.1), dimensions={0}, to_apply=%region_5.6 | reduce | flops 1572864 | bytes 5242882 | tf_op jit(solution)/shard_map/reduce_sum | solution.py:32
  170.1 5.1 %all-to-all-start.4 = ((bf16[8,64,1024]{2,1,0:T(8,128)(2,1)}), bf16[8,64,1024]{2,1,0:T(8,128)(2,1)S(1)}, u32[]{:S(2)}, u32[]{:S(2)}) async-start(bf16[8,64,1024]{2,1,0:T(8,128)(2,1)} %bitcast.17), calls=%async_computation.4 | async-start | bytes 2097152 | tf_op jit(solution)/shard_map/all_to_all | solution.py:20
  175.8 26.4 %all-to-all-done.4 = bf16[8,64,1024]{2,1,0:T(8,128)(2,1)S(1)} async-done(((bf16[8,64,1024]{2,1,0:T(8,128)(2,1)}), bf16[8,64,1024]{2,1,0:T(8,128)(2,1)S(1)}, u32[]{:S(2)}, u32[]{:S(2)}) %all-to-all-start.4) | async-done | bytes 1048608 | tf_op jit(solution)/shard_map/all_to_all | solution.py:20
  202.5 0.8 reshape.115
  203.3 8.9 %all-to-all-start.5 = ((bf16[24,16,128]{2,1,0:T(8,128)(2,1)}), bf16[24,16,128]{2,1,0:T(8,128)(2,1)S(1)}, u32[]{:S(2)}, u32[]{:S(2)}) async-start(bf16[24,16,128]{2,1,0:T(8,128)(2,1)} %reshape.115), calls=%async_computation.5 | async-start | bytes 196608 | tf_op jit(solution)/shard_map/all_to_all | solution.py:20
  212.3 11.0 %all-to-all-done.5 = bf16[24,16,128]{2,1,0:T(8,128)(2,1)S(1)} async-done(((bf16[24,16,128]{2,1,0:T(8,128)(2,1)}), bf16[24,16,128]{2,1,0:T(8,128)(2,1)S(1)}, u32[]{:S(2)}, u32[]{:S(2)}) %all-to-all-start.5) | async-done | bytes 98336 | tf_op jit(solution)/shard_map/all_to_all | solution.py:20
  223.4 1.3 gather_fusion.1
  224.7 1.5 multiply_reduce_fusion
  (52 shorter events, 5.8 us)
Async XLA Ops:
  0.0 109.7 %copy-start = (bf16[1,2048,176]{1,2,0:T(8,128)(2,1)S(1)}, bf16[1,2048,176]{1,2,0:T(8,128)(2,1)}, u32[]{:S(2)}) copy-start(bf16[1,2048,176]{1,2,0:T(8,128)(2,1)} %param.15) | copy-start | bytes 2162692
  69.5 4.8 %copy-start.1 = (bf16[1,176,2048]{2,1,0:T(8,128)(2,1)S(1)}, bf16[1,176,2048]{2,1,0:T(8,128)(2,1)}, u32[]{:S(2)}) copy-start(bf16[1,176,2048]{2,1,0:T(8,128)(2,1)} %param.17) | copy-start | bytes 2162692
  69.5 40.2 %all-to-all-start.2 = ((bf16[4,512,768]{2,1,0:T(8,128)(2,1)}), bf16[4,512,768]{2,1,0:T(8,128)(2,1)}, u32[]{:S(2)}, u32[]{:S(2)}) async-start(bf16[4,512,768]{2,1,0:T(8,128)(2,1)} %broadcast_in_dim.37), calls=%async_computation.2 | async-start | bytes 6291456 | tf_op jit(solution)/shard_map/all_to_all | solution.py:20
  74.8 1.7 copy-start.2
  76.1 0.9 copy-start.3
  165.7 9.8 %copy-start.4 = (s32[256,2]{0,1:T(2,128)S(1)}, s32[256,2]{0,1:T(2,128)}, u32[]{:S(2)}) copy-start(s32[256,2]{0,1:T(2,128)} %param.13) | copy-start | bytes 6148
  165.7 10.0 %copy-start.5 = (f32[256,2]{0,1:T(2,128)S(1)}, f32[256,2]{0,1:T(2,128)}, u32[]{:S(2)}) copy-start(f32[256,2]{0,1:T(2,128)} %param.14) | copy-start | bytes 6148
  170.1 42.2 %copy-start.6 = (f32[64]{0:T(128)S(1)}, f32[64]{0:T(128)}, u32[]{:S(2)}) copy-start(f32[64]{0:T(128)} %param.21) | copy-start | bytes 772
  170.1 32.1 %all-to-all-start.4 = ((bf16[8,64,1024]{2,1,0:T(8,128)(2,1)}), bf16[8,64,1024]{2,1,0:T(8,128)(2,1)S(1)}, u32[]{:S(2)}, u32[]{:S(2)}) async-start(bf16[8,64,1024]{2,1,0:T(8,128)(2,1)} %bitcast.17), calls=%async_computation.4 | async-start | bytes 2097152 | tf_op jit(solution)/shard_map/all_to_all | solution.py:20
  203.3 20.0 %all-to-all-start.5 = ((bf16[24,16,128]{2,1,0:T(8,128)(2,1)}), bf16[24,16,128]{2,1,0:T(8,128)(2,1)S(1)}, u32[]{:S(2)}, u32[]{:S(2)}) async-start(bf16[24,16,128]{2,1,0:T(8,128)(2,1)} %reshape.115), calls=%async_computation.5 | async-start | bytes 196608 | tf_op jit(solution)/shard_map/all_to_all | solution.py:20
